TPU v7x, 32 devices: a whole 2x2x4 slice. The times are simulated.
32 devices in a mesh: sp: 8 (over z, y), tp: 4 (over x, core).
Axes of the slice: x: 2, y: 2, z: 4, core: 2. Of those that a mesh axis runs over, the one named last changes fastest.
Arguments:
- inputs: bfloat16 [8192, 2048], P(('sp', 'tp')), may hold values from -90 to 90
- in_gain: float32 [2048], replicated, may hold values from 0.1 to 1.9
- w_query: bfloat16 [2048, 1024], replicated, may hold values from -2 to 2
- w_key: bfloat16 [2048, 128], replicated, may hold values from -2 to 2
- w_value: bfloat16 [2048, 128], replicated, may hold values from -0.125 to 0.125
- query_gain: float32 [64], replicated, may hold values from 0 to 8, as said below
- key_gain: float32 [64], replicated, may hold values from 0 to 8, as said below
- decay_sums: float32 [8192, 16], P('sp', 'tp'), may hold values from -1173 to 0, as said below
- w_out: bfloat16 [1024, 2048], replicated, may hold values from -0.1875 to 0.1875
Outputs:
- result: bfloat16 [8192, 2048], P(('sp', 'tp'))
Inputs may be any that keep to these rules, and one draw needn't show every extreme that they name: `decay_sums`: along positions, each head's entries never rise. `query_gain`: every entry is positive. `key_gain`: every entry is positive.
All inputs are finite; a program needn't handle non-finite values.
Results may differ from a plain program's by a relative error of at most 0.015.
The roundings to bfloat16 on the way count: a program that leaves them out, or rounds other values in their place, can miss the bound.
Values may be sent and summed in bfloat16 or wider, within the bound.
A program may use at most 64 MiB of HBM per device.

v0:
```python
from functools import partial
import math
import jax
import jax.numpy as jnp
from jax import lax
from jax.sharding import PartitionSpec as P

epsilon = 1e-06


def rms_norm(vector, gain_vec):
    return (
        vector * lax.rsqrt(jnp.mean(vector * vector, axis=-1, keepdims=True) + epsilon) * gain_vec
    )


def attend_step(
    masked, query_rows, query_decay, query_pos, key_slice, value_slice, decay_slice, key_pos, inner
):
    peak, total, weighted = inner
    score_scale = query_rows.shape[2] ** (-0.5)
    scores = (
        jnp.einsum("thd,ud->htu", query_rows, key_slice, preferred_element_type=jnp.float32)
        * score_scale
    )
    scores = scores + query_decay[:, :, None] - decay_slice[:, None, :]
    if masked:
        visible = key_pos[None, :] <= query_pos[:, None]
        scores = jnp.where(visible[None], scores, -1e30)
    peak_new = jnp.maximum(peak, jnp.max(scores, axis=-1))
    weights_exp = jnp.exp(scores - peak_new[:, :, None])
    if masked:
        weights_exp = jnp.where(visible[None], weights_exp, 0.0)
    rescale = jnp.exp(peak - peak_new)
    total_new = total * rescale + jnp.sum(weights_exp, axis=-1)
    product = jnp.einsum(
        "htu,ud->thd",
        weights_exp.astype(jnp.bfloat16),
        value_slice,
        preferred_element_type=jnp.float32,
    )
    weighted_new = weighted * rescale.T[:, :, None] + product
    return (peak_new, total_new, weighted_new)


def keep_state(inner):
    return inner


def per_device(inputs, in_gain, w_query, w_key, w_value, query_gain, key_gain, decay_sums, w_out):
    tp_count = lax.axis_size("tp")
    sp_rank = lax.axis_index("sp")
    heads_dev = decay_sums.shape[1]
    head_size = query_gain.shape[0]
    kv_heads = w_key.shape[1] // head_size
    width_dev = heads_dev * head_size
    normed = rms_norm(inputs.astype(jnp.float32), in_gain).astype(jnp.bfloat16)
    row_count = normed.shape[0]
    all_heads = w_query.shape[1] // head_size
    query_all = rms_norm(
        jnp.dot(normed, w_query, preferred_element_type=jnp.float32).reshape(
            row_count, all_heads, head_size
        ),
        query_gain,
    ).astype(jnp.bfloat16)
    key_all = rms_norm(
        jnp.dot(normed, w_key, preferred_element_type=jnp.float32).reshape(
            row_count, kv_heads, head_size
        ),
        key_gain,
    ).astype(jnp.bfloat16)
    value_all = (
        jnp.dot(normed, w_value, preferred_element_type=jnp.float32)
        .astype(jnp.bfloat16)
        .reshape(row_count, kv_heads, head_size)
    )
    pair_all = jnp.repeat(
        jnp.concatenate([key_all, value_all], axis=2), tp_count // kv_heads, axis=1
    )
    packed = jnp.concatenate([query_all.reshape(row_count, tp_count, width_dev), pair_all], axis=2)
    received = lax.all_to_all(packed, "tp", split_axis=1, concat_axis=0, tiled=True)[:, 0]
    tok_rows = received.shape[0]
    queries = received[:, :width_dev].reshape(tok_rows, heads_dev, head_size)
    key_values = received[:, width_dev:]
    all_decays = lax.all_gather(decay_sums, "sp", axis=0, tiled=True)
    groups = (queries, sp_rank * tok_rows)
    prepared = []
    query_rows, first_pos = groups
    rows = query_rows.shape[0]
    query_decay = lax.dynamic_slice_in_dim(all_decays, first_pos, rows, 0).T
    query_pos = first_pos + jnp.arange(rows, dtype=jnp.int32)
    prepared.append((query_rows, query_decay, query_pos, first_pos, first_pos + rows - 1))
    initial = tuple(
        (
            (
                jnp.full((heads_dev, entry[0].shape[0]), -1e30, jnp.float32),
                jnp.zeros((heads_dev, entry[0].shape[0]), jnp.float32),
                jnp.zeros((entry[0].shape[0], heads_dev, head_size), jnp.float32),
            )
            for entry in prepared
        )
    )
    state = initial
    pieces = lax.all_gather(key_values, "sp", axis=0, tiled=True)
    piece_rows = pieces.shape[0]
    key_block = math.gcd(piece_rows, 512)

    def one_block(carry, block_index):
        key_start = block_index * key_block
        pair_slice = lax.dynamic_slice_in_dim(pieces, block_index * key_block, key_block, 0)
        key_slice = pair_slice[:, :head_size]
        value_slice = pair_slice[:, head_size:]
        decay_slice = lax.dynamic_slice_in_dim(all_decays, key_start, key_block, 0).T
        key_pos = key_start + jnp.arange(key_block, dtype=jnp.int32)
        updated = []
        for (query_rows, query_decay, query_pos, first_pos, last_pos), inner in zip(
            prepared, carry
        ):
            branch = jnp.where(
                key_start > last_pos, 0, jnp.where(key_start + key_block - 1 <= first_pos, 1, 2)
            )
            full_step = partial(
                attend_step,
                False,
                query_rows,
                query_decay,
                query_pos,
                key_slice,
                value_slice,
                decay_slice,
                key_pos,
            )
            masked_step = partial(
                attend_step,
                True,
                query_rows,
                query_decay,
                query_pos,
                key_slice,
                value_slice,
                decay_slice,
                key_pos,
            )
            updated.append(lax.switch(branch, [keep_state, full_step, masked_step], inner))
        return (tuple(updated), None)

    state, unused = lax.scan(one_block, state, jnp.arange(piece_rows // key_block, dtype=jnp.int32))
    outputs = [
        (weighted / total.T[:, :, None]).astype(jnp.bfloat16) for peak, total, weighted in state
    ]
    attended = outputs[0].reshape(tok_rows, width_dev)
    out_rows = lax.all_to_all(attended, "tp", split_axis=0, concat_axis=1, tiled=True)
    result = jnp.dot(out_rows, w_out, preferred_element_type=jnp.float32).astype(jnp.bfloat16)
    return result


def solution(mesh):
    placed = (P(("sp", "tp"), None), P(), P(), P(), P(), P(), P(), P("sp", "tp"), P())
    return jax.shard_map(
        per_device, mesh=mesh, in_specs=placed, out_specs=P(("sp", "tp"), None), check_vma=False
    )
```

profile of v0, /device:TPU:28, one launch (start us, length us, event | category | flops | bytes accessed | tf_op | source)
XLA Modules:
  0.0 254.3 jit_solution(247003745765237062)
XLA Ops:
  11.9 4.8 %fusion.51 = (f32[256,1024]{1,0:T(8,128)}, f32[256,1024]{1,0:T(8,128)S(1)}) fusion(bf16[2048,1024]{1,0:T(8,128)(2,1)} %param.16, bf16[256,2048]{1,0:T(8,128)(2,1)} %param.14, f32[2048]{0:T(1024)} %param.15, f32[256]{0:T(256)S(1)} %add_rsqrt_fusion.2), kind=kOutput, calls=%fused_computation.65 | convolution fusion | flops 1076101120 | bytes 7349248 | tf_op jit(solution)/shard_map/dot_general | solution.py:61
  19.3 14.2 %all_to_all.34 = bf16[256,4,384]{0,2,1:T(8,128)(2,1)S(1)} all-to-all(bf16[256,4,384]{0,2,1:T(8,128)(2,1)S(1)} %pad_maximum_fusion), channel_id=1, replica_groups=mesh['sp'=8,'tp'=4] {'tp'}, dimensions={1} | all-to-all | bytes 1572864 | tf_op jit(solution)/shard_map/all_to_all | solution.py:81
  34.6 31.2 %all_gather.7 = f32[8192,4]{0,1:T(4,128)S(1)} all-gather(f32[1024,4]{0,1:T(4,128)S(1)} %copy-done.1), channel_id=1, replica_groups=mesh['sp'=8,'tp'=4] {'sp'}, dimensions={0}, use_global_device_ids=true | all-gather | bytes 147456 | tf_op jit(solution)/shard_map/all_gather | solution.py:85
  66.1 15.7 %all-gather.2.cloned.1.call-done = bf16[8192,128]{1,0:T(8,128)(2,1)} async-done(((bf16[1024,128]{1,0:T(8,128)(2,1)}), bf16[8192,128]{1,0:T(8,128)(2,1)}) %all-gather.2.cloned.1.call-update) | async-done | bytes 2097168 | tf_op jit(solution)/shard_map/all_gather | solution.py:104
  81.9 149.1 %while.20 = (s32[]{:T(128)}, f32[4,1024]{1,0:T(4,128)S(1)}, f32[4,1024]{1,0:T(4,128)S(1)}, f32[1024,4,64]{0,2,1:T(8,128)S(1)}, s32[16]{0:T(128)S(1)}, /*index=5*...) while((s32[]{:T(128)}, f32[4,1024]{1,0:T(4,128)S(1)}, ...), condition=%wide.region_11.12_spmd.clone.clone, body=%wide.region_3.11_spmd.clone.clone.sunk | while | flops 577779200 | bytes 30917152 | solution.py:147
  84.5 6.3 %conditional.4 = ((f32[4,1024]{1,0:T(4,128)S(1)}, f32[4,1024]{1,0:T(4,128)S(1)}, f32[1024,4,64]{0,2,1:T(8,128)S(1)})) conditional(s32[]{:T(128)} %clamp.12, (f32[4,1024]{1,0:T(4,128)S(1)}, f32[4,1024]{1,0:T(4,128)S(1)}, f32[1024,4,64]{0,2,1:T(8,128)S(1)}) %tuple.72, (bf16[512,64]{0,1:T(8,128)(2,1)S(1)}, ...), branch_computations={%region_4.4_spmd, %region_5.7_spmd, %region_8.10_spmd} | conditional | flops 577779200 | bytes 30369832 | solution.py:144
  93.5 6.3 %conditional.4 = ((f32[4,1024]{1,0:T(4,128)S(1)}, f32[4,1024]{1,0:T(4,128)S(1)}, f32[1024,4,64]{0,2,1:T(8,128)S(1)})) conditional(s32[]{:T(128)} %clamp.12, (f32[4,1024]{1,0:T(4,128)S(1)}, f32[4,1024]{1,0:T(4,128)S(1)}, f32[1024,4,64]{0,2,1:T(8,128)S(1)}) %tuple.72, (bf16[512,64]{0,1:T(8,128)(2,1)S(1)}, ...), branch_computations={%region_4.4_spmd, %region_5.7_spmd, %region_8.10_spmd} | conditional | flops 577779200 | bytes 30369832 | solution.py:144
  102.5 6.3 %conditional.4 = ((f32[4,1024]{1,0:T(4,128)S(1)}, f32[4,1024]{1,0:T(4,128)S(1)}, f32[1024,4,64]{0,2,1:T(8,128)S(1)})) conditional(s32[]{:T(128)} %clamp.12, (f32[4,1024]{1,0:T(4,128)S(1)}, f32[4,1024]{1,0:T(4,128)S(1)}, f32[1024,4,64]{0,2,1:T(8,128)S(1)}) %tuple.72, (bf16[512,64]{0,1:T(8,128)(2,1)S(1)}, ...), branch_computations={%region_4.4_spmd, %region_5.7_spmd, %region_8.10_spmd} | conditional | flops 577779200 | bytes 30369832 | solution.py:144
  111.5 6.3 %conditional.4 = ((f32[4,1024]{1,0:T(4,128)S(1)}, f32[4,1024]{1,0:T(4,128)S(1)}, f32[1024,4,64]{0,2,1:T(8,128)S(1)})) conditional(s32[]{:T(128)} %clamp.12, (f32[4,1024]{1,0:T(4,128)S(1)}, f32[4,1024]{1,0:T(4,128)S(1)}, f32[1024,4,64]{0,2,1:T(8,128)S(1)}) %tuple.72, (bf16[512,64]{0,1:T(8,128)(2,1)S(1)}, ...), branch_computations={%region_4.4_spmd, %region_5.7_spmd, %region_8.10_spmd} | conditional | flops 577779200 | bytes 30369832 | solution.py:144
  120.4 6.3 %conditional.4 = ((f32[4,1024]{1,0:T(4,128)S(1)}, f32[4,1024]{1,0:T(4,128)S(1)}, f32[1024,4,64]{0,2,1:T(8,128)S(1)})) conditional(s32[]{:T(128)} %clamp.12, (f32[4,1024]{1,0:T(4,128)S(1)}, f32[4,1024]{1,0:T(4,128)S(1)}, f32[1024,4,64]{0,2,1:T(8,128)S(1)}) %tuple.72, (bf16[512,64]{0,1:T(8,128)(2,1)S(1)}, ...), branch_computations={%region_4.4_spmd, %region_5.7_spmd, %region_8.10_spmd} | conditional | flops 577779200 | bytes 30369832 | solution.py:144
  129.4 6.3 %conditional.4 = ((f32[4,1024]{1,0:T(4,128)S(1)}, f32[4,1024]{1,0:T(4,128)S(1)}, f32[1024,4,64]{0,2,1:T(8,128)S(1)})) conditional(s32[]{:T(128)} %clamp.12, (f32[4,1024]{1,0:T(4,128)S(1)}, f32[4,1024]{1,0:T(4,128)S(1)}, f32[1024,4,64]{0,2,1:T(8,128)S(1)}) %tuple.72, (bf16[512,64]{0,1:T(8,128)(2,1)S(1)}, ...), branch_computations={%region_4.4_spmd, %region_5.7_spmd, %region_8.10_spmd} | conditional | flops 577779200 | bytes 30369832 | solution.py:144
  138.4 6.3 %conditional.4 = ((f32[4,1024]{1,0:T(4,128)S(1)}, f32[4,1024]{1,0:T(4,128)S(1)}, f32[1024,4,64]{0,2,1:T(8,128)S(1)})) conditional(s32[]{:T(128)} %clamp.12, (f32[4,1024]{1,0:T(4,128)S(1)}, f32[4,1024]{1,0:T(4,128)S(1)}, f32[1024,4,64]{0,2,1:T(8,128)S(1)}) %tuple.72, (bf16[512,64]{0,1:T(8,128)(2,1)S(1)}, ...), branch_computations={%region_4.4_spmd, %region_5.7_spmd, %region_8.10_spmd} | conditional | flops 577779200 | bytes 30369832 | solution.py:144
  147.4 6.3 %conditional.4 = ((f32[4,1024]{1,0:T(4,128)S(1)}, f32[4,1024]{1,0:T(4,128)S(1)}, f32[1024,4,64]{0,2,1:T(8,128)S(1)})) conditional(s32[]{:T(128)} %clamp.12, (f32[4,1024]{1,0:T(4,128)S(1)}, f32[4,1024]{1,0:T(4,128)S(1)}, f32[1024,4,64]{0,2,1:T(8,128)S(1)}) %tuple.72, (bf16[512,64]{0,1:T(8,128)(2,1)S(1)}, ...), branch_computations={%region_4.4_spmd, %region_5.7_spmd, %region_8.10_spmd} | conditional | flops 577779200 | bytes 30369832 | solution.py:144
  156.3 6.3 %conditional.4 = ((f32[4,1024]{1,0:T(4,128)S(1)}, f32[4,1024]{1,0:T(4,128)S(1)}, f32[1024,4,64]{0,2,1:T(8,128)S(1)})) conditional(s32[]{:T(128)} %clamp.12, (f32[4,1024]{1,0:T(4,128)S(1)}, f32[4,1024]{1,0:T(4,128)S(1)}, f32[1024,4,64]{0,2,1:T(8,128)S(1)}) %tuple.72, (bf16[512,64]{0,1:T(8,128)(2,1)S(1)}, ...), branch_computations={%region_4.4_spmd, %region_5.7_spmd, %region_8.10_spmd} | conditional | flops 577779200 | bytes 30369832 | solution.py:144
  165.3 6.3 %conditional.4 = ((f32[4,1024]{1,0:T(4,128)S(1)}, f32[4,1024]{1,0:T(4,128)S(1)}, f32[1024,4,64]{0,2,1:T(8,128)S(1)})) conditional(s32[]{:T(128)} %clamp.12, (f32[4,1024]{1,0:T(4,128)S(1)}, f32[4,1024]{1,0:T(4,128)S(1)}, f32[1024,4,64]{0,2,1:T(8,128)S(1)}) %tuple.72, (bf16[512,64]{0,1:T(8,128)(2,1)S(1)}, ...), branch_computations={%region_4.4_spmd, %region_5.7_spmd, %region_8.10_spmd} | conditional | flops 577779200 | bytes 30369832 | solution.py:144
  174.3 6.3 %conditional.4 = ((f32[4,1024]{1,0:T(4,128)S(1)}, f32[4,1024]{1,0:T(4,128)S(1)}, f32[1024,4,64]{0,2,1:T(8,128)S(1)})) conditional(s32[]{:T(128)} %clamp.12, (f32[4,1024]{1,0:T(4,128)S(1)}, f32[4,1024]{1,0:T(4,128)S(1)}, f32[1024,4,64]{0,2,1:T(8,128)S(1)}) %tuple.72, (bf16[512,64]{0,1:T(8,128)(2,1)S(1)}, ...), branch_computations={%region_4.4_spmd, %region_5.7_spmd, %region_8.10_spmd} | conditional | flops 577779200 | bytes 30369832 | solution.py:144
  183.3 6.3 %conditional.4 = ((f32[4,1024]{1,0:T(4,128)S(1)}, f32[4,1024]{1,0:T(4,128)S(1)}, f32[1024,4,64]{0,2,1:T(8,128)S(1)})) conditional(s32[]{:T(128)} %clamp.12, (f32[4,1024]{1,0:T(4,128)S(1)}, f32[4,1024]{1,0:T(4,128)S(1)}, f32[1024,4,64]{0,2,1:T(8,128)S(1)}) %tuple.72, (bf16[512,64]{0,1:T(8,128)(2,1)S(1)}, ...), branch_computations={%region_4.4_spmd, %region_5.7_spmd, %region_8.10_spmd} | conditional | flops 577779200 | bytes 30369832 | solution.py:144
  192.3 6.3 %conditional.4 = ((f32[4,1024]{1,0:T(4,128)S(1)}, f32[4,1024]{1,0:T(4,128)S(1)}, f32[1024,4,64]{0,2,1:T(8,128)S(1)})) conditional(s32[]{:T(128)} %clamp.12, (f32[4,1024]{1,0:T(4,128)S(1)}, f32[4,1024]{1,0:T(4,128)S(1)}, f32[1024,4,64]{0,2,1:T(8,128)S(1)}) %tuple.72, (bf16[512,64]{0,1:T(8,128)(2,1)S(1)}, ...), branch_computations={%region_4.4_spmd, %region_5.7_spmd, %region_8.10_spmd} | conditional | flops 577779200 | bytes 30369832 | solution.py:144
  201.2 6.3 %conditional.4 = ((f32[4,1024]{1,0:T(4,128)S(1)}, f32[4,1024]{1,0:T(4,128)S(1)}, f32[1024,4,64]{0,2,1:T(8,128)S(1)})) conditional(s32[]{:T(128)} %clamp.12, (f32[4,1024]{1,0:T(4,128)S(1)}, f32[4,1024]{1,0:T(4,128)S(1)}, f32[1024,4,64]{0,2,1:T(8,128)S(1)}) %tuple.72, (bf16[512,64]{0,1:T(8,128)(2,1)S(1)}, ...), branch_computations={%region_4.4_spmd, %region_5.7_spmd, %region_8.10_spmd} | conditional | flops 577779200 | bytes 30369832 | solution.py:144
  210.2 9.1 %conditional.4 = ((f32[4,1024]{1,0:T(4,128)S(1)}, f32[4,1024]{1,0:T(4,128)S(1)}, f32[1024,4,64]{0,2,1:T(8,128)S(1)})) conditional(s32[]{:T(128)} %clamp.12, (f32[4,1024]{1,0:T(4,128)S(1)}, f32[4,1024]{1,0:T(4,128)S(1)}, f32[1024,4,64]{0,2,1:T(8,128)S(1)}) %tuple.72, (bf16[512,64]{0,1:T(8,128)(2,1)S(1)}, ...), branch_computations={%region_4.4_spmd, %region_5.7_spmd, %region_8.10_spmd} | conditional | flops 577779200 | bytes 30369832 | solution.py:144
  213.0 3.2 %fusion.30 = f32[1024,4,64]{0,2,1:T(8,128)S(1)} fusion(f32[512,1024,4]{1,0,2:T(8,128)S(1)} %get-tuple-element.451, f32[4,1024]{1,0:T(4,128)S(1)} %get-tuple-element.541, f32[4,512]{1,0:T(4,128)S(1)} %get-tuple-element.303, f32[4,1024]{1,0:T(4,128)S(1)} %get-tuple-element.302, pred[1024,512]{0,1:T(8,128)(4,1)S(1)} %broadcast_compare_fusion, ...), kind=kOutput, calls=%fused_computation.27 | convolution fusion | flops 283639808 | bytes 11132928 | tf_op jit(solution)/shard_map/while/body/eval_jaxpr/cond/branch_2_fun/htu,ud->thd/dot_general | solution.py:36
  221.9 9.1 %conditional.4 = ((f32[4,1024]{1,0:T(4,128)S(1)}, f32[4,1024]{1,0:T(4,128)S(1)}, f32[1024,4,64]{0,2,1:T(8,128)S(1)})) conditional(s32[]{:T(128)} %clamp.12, (f32[4,1024]{1,0:T(4,128)S(1)}, f32[4,1024]{1,0:T(4,128)S(1)}, f32[1024,4,64]{0,2,1:T(8,128)S(1)}) %tuple.72, (bf16[512,64]{0,1:T(8,128)(2,1)S(1)}, ...), branch_computations={%region_4.4_spmd, %region_5.7_spmd, %region_8.10_spmd} | conditional | flops 577779200 | bytes 30369832 | solution.py:144
  231.6 11.5 %all_to_all.35 = bf16[4,256,256]{1,2,0:T(8,128)(2,1)S(1)} all-to-all(bf16[4,256,256]{1,2,0:T(8,128)(2,1)S(1)} %copy.41), channel_id=1, replica_groups=mesh['sp'=8,'tp'=4] {'tp'}, dimensions={0} | all-to-all | bytes 1048576 | tf_op jit(solution)/shard_map/all_to_all | solution.py:152
  243.1 4.4 %convolution_convert_fusion = bf16[256,2048]{1,0:T(8,128)(2,1)} fusion(bf16[256,1024]{0,1:T(8,128)(2,1)S(1)} %bitcast.110, bf16[1024,2048]{1,0:T(8,128)(2,1)} %param.22), kind=kOutput, calls=%fused_computation.44 | convolution fusion | flops 1074266112 | bytes 5767168 | tf_op jit(solution)/shard_map/dot_general | solution.py:153
  (252 shorter events, 142.8 us)
Async XLA Ops:
  6.5 1.6 copy-start
  6.5 75.2 %all-gather.2.cloned.1.call-start = ((), (), s32[]{:S(2)}) async-start(), calls=%async_computation.2 | async-start | bytes 2359296 | tf_op jit(solution)/shard_map/all_gather | solution.py:104
  8.1 10.6 %copy-start.3 = (f32[64]{0:T(128)S(1)}, f32[64]{0:T(128)}, u32[]{:S(2)}) copy-start(f32[64]{0:T(128)} %param.19) | copy-start | bytes 772
  8.1 10.7 %copy-start.2 = (f32[64]{0:T(128)S(1)}, f32[64]{0:T(128)}, u32[]{:S(2)}) copy-start(f32[64]{0:T(128)} %param.20) | copy-start | bytes 772
  16.7 17.9 %copy-start.1 = (f32[1024,4]{0,1:T(4,128)S(1)}, f32[1024,4]{0,1:T(4,128)}, u32[]{:S(2)}) copy-start(f32[1024,4]{0,1:T(4,128)} %param.21) | copy-start | bytes 49156
Sparse Core Ops, SparseCore 0:
  34.7 46.9 all-gather.1
where the time goes:
time: 255 us; the launch traced here: 254 us
  matrix products  82.4 us (32%)
  blocking collectives  56.9 us (22%)
  other arithmetic  38.4 us (15%)
  local copies, waits for them, and re-layouts  34.4 us (13%)
  waiting for transfers between devices  15.7 us (6%)
  between operations  13.6 us (5%)
  loops' own time  13 us (5%)
    dot_general x16, matrix products, attend_step(): jnp.einsum('htu,ud->thd', weights_exp.astype(jnp.bfloat16), value_slice,...  42.9 us
    reduce_sum x16, other arithmetic, attend_step(): total_new = total * rescale + jnp.sum(weights_exp, axis=-1)  35 us
    all_gather x1, blocking collectives, per_device(): all_decays = lax.all_gather(decay_sums, 'sp', axis=0, tiled=True)  31.2 us
    dot_general x16, matrix products, attend_step(): jnp.einsum('thd,ud->htu', query_rows, key_slice, preferred_element_type=j...  26.4 us
    slice x16, local copies, waits for them, and re-layouts, one_block(): value_slice = pair_slice[:, head_size:]  17.6 us
    all_gather x1, waiting for transfers between devices, per_device(): pieces = lax.all_gather(key_values, 'sp', axis=0, tiled=True)  15.7 us
    all_to_all x1, blocking collectives, per_device(): lax.all_to_all(packed, 'tp', split_axis=1, concat_axis=0, tiled=True)[:, 0]  14.2 us
    another operation x1, loops' own time, per_device(): lax.scan(one_block, state, jnp.arange(piece_rows // key_block, dtype=jnp....  11.8 us
  transfers between devices with their start and end apart: 1, of which 1 were waited for; matrix products, arithmetic and copies ran while one was open for 0% of the time, Pallas kernels for 0%

commit v1 on v0

--- a/solution.py
+++ b/solution.py
@@ -78,7 +78,10 @@
         jnp.concatenate([key_all, value_all], axis=2), tp_count // kv_heads, axis=1
     )
     packed = jnp.concatenate([query_all.reshape(row_count, tp_count, width_dev), pair_all], axis=2)
-    received = lax.all_to_all(packed, "tp", split_axis=1, concat_axis=0, tiled=True)[:, 0]
+    received = jnp.concatenate(
+        lax.all_to_all(jnp.stack(jnp.split(packed, lax.axis_size("tp"), axis=1)), "tp", 0, 0),
+        axis=0,
+    )[:, 0]
     tok_rows = received.shape[0]
     queries = received[:, :width_dev].reshape(tok_rows, heads_dev, head_size)
     key_values = received[:, width_dev:]

time: 255 us -> 257 us (level)
  no operation moved by 1% of the time
where the time goes in v1:
time: 257 us; the launch traced here: 256 us
  matrix products  83.8 us (33%)
  blocking collectives  56.8 us (22%)
  other arithmetic  39.2 us (15%)
  local copies, waits for them, and re-layouts  34.4 us (13%)
  waiting for transfers between devices  15.7 us (6%)
  between operations  13.6 us (5%)
  loops' own time  13 us (5%)
    dot_general x16, matrix products, attend_step(): jnp.einsum('htu,ud->thd', weights_exp.astype(jnp.bfloat16), value_slice,...  44 us
    reduce_sum x16, other arithmetic, attend_step(): total_new = total * rescale + jnp.sum(weights_exp, axis=-1)  35.6 us
    all_gather x1, blocking collectives, per_device(): all_decays = lax.all_gather(decay_sums, 'sp', axis=0, tiled=True)  31.2 us
    dot_general x16, matrix products, attend_step(): jnp.einsum('thd,ud->htu', query_rows, key_slice, preferred_element_type=j...  26.8 us
    slice x16, local copies, waits for them, and re-layouts, one_block(): value_slice = pair_slice[:, head_size:]  17.6 us
    all_gather x1, waiting for transfers between devices, per_device(): pieces = lax.all_gather(key_values, 'sp', axis=0, tiled=True)  15.6 us
    all_to_all x1, blocking collectives, per_device(): lax.all_to_all(jnp.stack(jnp.split(packed, lax.axis_size('tp'), axis=1)),...  14.2 us
    another operation x1, loops' own time, per_device(): lax.scan(one_block, state, jnp.arange(piece_rows // key_block, dtype=jnp....  11.8 us
  transfers between devices with their start and end apart: 1, of which 1 were waited for; matrix products, arithmetic and copies ran while one was open for 0% of the time, Pallas kernels for 0%

profile of v1, /device:TPU:28, one launch (start us, length us, event | category | flops | bytes accessed | tf_op | source)
XLA Modules:
  0.0 256.4 jit_solution(733963940798986127)
XLA Ops:
  11.9 4.8 %fusion.58 = (f32[256,1024]{1,0:T(8,128)}, f32[256,1024]{1,0:T(8,128)S(1)}) fusion(bf16[2048,1024]{1,0:T(8,128)(2,1)} %param.16, bf16[256,2048]{1,0:T(8,128)(2,1)} %param.14, f32[2048]{0:T(1024)} %param.15, f32[256]{0:T(256)S(1)} %add_rsqrt_fusion.2), kind=kOutput, calls=%fused_computation.79 | convolution fusion | flops 1076101120 | bytes 7349248 | tf_op jit(solution)/shard_map/dot_general | solution.py:61
  19.5 14.2 %all_to_all.24 = bf16[4,256,1,384]{1,3,2,0:T(8,128)(2,1)S(1)} all-to-all(bf16[4,256,1,384]{1,3,2,0:T(8,128)(2,1)S(1)} %pad_maximum_fusion), channel_id=1, replica_groups=mesh['sp'=8,'tp'=4] {'tp'}, dimensions={0} | all-to-all | bytes 1572864 | tf_op jit(solution)/shard_map/all_to_all | solution.py:82
  34.8 31.2 %all_gather.7 = f32[8192,4]{0,1:T(4,128)S(1)} all-gather(f32[1024,4]{0,1:T(4,128)S(1)} %copy-done.1), channel_id=1, replica_groups=mesh['sp'=8,'tp'=4] {'sp'}, dimensions={0}, use_global_device_ids=true | all-gather | bytes 147456 | tf_op jit(solution)/shard_map/all_gather | solution.py:88
  66.3 15.6 %all-gather.2.cloned.1.call-done = bf16[8192,128]{1,0:T(8,128)(2,1)} async-done(((bf16[1024,128]{1,0:T(8,128)(2,1)}), bf16[8192,128]{1,0:T(8,128)(2,1)}) %all-gather.2.cloned.1.call-update) | async-done | bytes 2097168 | tf_op jit(solution)/shard_map/all_gather | solution.py:107
  82.0 151.1 %while.20 = (s32[]{:T(128)}, f32[4,1024]{1,0:T(4,128)S(1)}, f32[4,1024]{1,0:T(4,128)S(1)}, f32[1024,4,64]{0,2,1:T(8,128)S(1)}, s32[16]{0:T(128)S(1)}, /*index=5*...) while((s32[]{:T(128)}, f32[4,1024]{1,0:T(4,128)S(1)}, ...), condition=%wide.region_11.12_spmd.clone.clone, body=%wide.region_3.11_spmd.clone.clone.sunk | while | flops 577779200 | bytes 30917152 | solution.py:150
  84.7 6.4 %conditional.4 = ((f32[4,1024]{1,0:T(4,128)S(1)}, f32[4,1024]{1,0:T(4,128)S(1)}, f32[1024,4,64]{0,2,1:T(8,128)S(1)})) conditional(s32[]{:T(128)} %clamp.12, (f32[4,1024]{1,0:T(4,128)S(1)}, f32[4,1024]{1,0:T(4,128)S(1)}, f32[1024,4,64]{0,2,1:T(8,128)S(1)}) %tuple.75, (bf16[512,64]{0,1:T(8,128)(2,1)S(1)}, ...), branch_computations={%region_4.4_spmd, %region_5.7_spmd, %region_8.10_spmd} | conditional | flops 577779200 | bytes 30369832 | solution.py:147
  93.8 6.4 %conditional.4 = ((f32[4,1024]{1,0:T(4,128)S(1)}, f32[4,1024]{1,0:T(4,128)S(1)}, f32[1024,4,64]{0,2,1:T(8,128)S(1)})) conditional(s32[]{:T(128)} %clamp.12, (f32[4,1024]{1,0:T(4,128)S(1)}, f32[4,1024]{1,0:T(4,128)S(1)}, f32[1024,4,64]{0,2,1:T(8,128)S(1)}) %tuple.75, (bf16[512,64]{0,1:T(8,128)(2,1)S(1)}, ...), branch_computations={%region_4.4_spmd, %region_5.7_spmd, %region_8.10_spmd} | conditional | flops 577779200 | bytes 30369832 | solution.py:147
  102.8 6.4 %conditional.4 = ((f32[4,1024]{1,0:T(4,128)S(1)}, f32[4,1024]{1,0:T(4,128)S(1)}, f32[1024,4,64]{0,2,1:T(8,128)S(1)})) conditional(s32[]{:T(128)} %clamp.12, (f32[4,1024]{1,0:T(4,128)S(1)}, f32[4,1024]{1,0:T(4,128)S(1)}, f32[1024,4,64]{0,2,1:T(8,128)S(1)}) %tuple.75, (bf16[512,64]{0,1:T(8,128)(2,1)S(1)}, ...), branch_computations={%region_4.4_spmd, %region_5.7_spmd, %region_8.10_spmd} | conditional | flops 577779200 | bytes 30369832 | solution.py:147
  111.9 6.4 %conditional.4 = ((f32[4,1024]{1,0:T(4,128)S(1)}, f32[4,1024]{1,0:T(4,128)S(1)}, f32[1024,4,64]{0,2,1:T(8,128)S(1)})) conditional(s32[]{:T(128)} %clamp.12, (f32[4,1024]{1,0:T(4,128)S(1)}, f32[4,1024]{1,0:T(4,128)S(1)}, f32[1024,4,64]{0,2,1:T(8,128)S(1)}) %tuple.75, (bf16[512,64]{0,1:T(8,128)(2,1)S(1)}, ...), branch_computations={%region_4.4_spmd, %region_5.7_spmd, %region_8.10_spmd} | conditional | flops 577779200 | bytes 30369832 | solution.py:147
  121.0 6.4 %conditional.4 = ((f32[4,1024]{1,0:T(4,128)S(1)}, f32[4,1024]{1,0:T(4,128)S(1)}, f32[1024,4,64]{0,2,1:T(8,128)S(1)})) conditional(s32[]{:T(128)} %clamp.12, (f32[4,1024]{1,0:T(4,128)S(1)}, f32[4,1024]{1,0:T(4,128)S(1)}, f32[1024,4,64]{0,2,1:T(8,128)S(1)}) %tuple.75, (bf16[512,64]{0,1:T(8,128)(2,1)S(1)}, ...), branch_computations={%region_4.4_spmd, %region_5.7_spmd, %region_8.10_spmd} | conditional | flops 577779200 | bytes 30369832 | solution.py:147
  130.1 6.4 %conditional.4 = ((f32[4,1024]{1,0:T(4,128)S(1)}, f32[4,1024]{1,0:T(4,128)S(1)}, f32[1024,4,64]{0,2,1:T(8,128)S(1)})) conditional(s32[]{:T(128)} %clamp.12, (f32[4,1024]{1,0:T(4,128)S(1)}, f32[4,1024]{1,0:T(4,128)S(1)}, f32[1024,4,64]{0,2,1:T(8,128)S(1)}) %tuple.75, (bf16[512,64]{0,1:T(8,128)(2,1)S(1)}, ...), branch_computations={%region_4.4_spmd, %region_5.7_spmd, %region_8.10_spmd} | conditional | flops 577779200 | bytes 30369832 | solution.py:147
  139.1 6.4 %conditional.4 = ((f32[4,1024]{1,0:T(4,128)S(1)}, f32[4,1024]{1,0:T(4,128)S(1)}, f32[1024,4,64]{0,2,1:T(8,128)S(1)})) conditional(s32[]{:T(128)} %clamp.12, (f32[4,1024]{1,0:T(4,128)S(1)}, f32[4,1024]{1,0:T(4,128)S(1)}, f32[1024,4,64]{0,2,1:T(8,128)S(1)}) %tuple.75, (bf16[512,64]{0,1:T(8,128)(2,1)S(1)}, ...), branch_computations={%region_4.4_spmd, %region_5.7_spmd, %region_8.10_spmd} | conditional | flops 577779200 | bytes 30369832 | solution.py:147
  148.2 6.4 %conditional.4 = ((f32[4,1024]{1,0:T(4,128)S(1)}, f32[4,1024]{1,0:T(4,128)S(1)}, f32[1024,4,64]{0,2,1:T(8,128)S(1)})) conditional(s32[]{:T(128)} %clamp.12, (f32[4,1024]{1,0:T(4,128)S(1)}, f32[4,1024]{1,0:T(4,128)S(1)}, f32[1024,4,64]{0,2,1:T(8,128)S(1)}) %tuple.75, (bf16[512,64]{0,1:T(8,128)(2,1)S(1)}, ...), branch_computations={%region_4.4_spmd, %region_5.7_spmd, %region_8.10_spmd} | conditional | flops 577779200 | bytes 30369832 | solution.py:147
  157.3 6.4 %conditional.4 = ((f32[4,1024]{1,0:T(4,128)S(1)}, f32[4,1024]{1,0:T(4,128)S(1)}, f32[1024,4,64]{0,2,1:T(8,128)S(1)})) conditional(s32[]{:T(128)} %clamp.12, (f32[4,1024]{1,0:T(4,128)S(1)}, f32[4,1024]{1,0:T(4,128)S(1)}, f32[1024,4,64]{0,2,1:T(8,128)S(1)}) %tuple.75, (bf16[512,64]{0,1:T(8,128)(2,1)S(1)}, ...), branch_computations={%region_4.4_spmd, %region_5.7_spmd, %region_8.10_spmd} | conditional | flops 577779200 | bytes 30369832 | solution.py:147
  166.4 6.4 %conditional.4 = ((f32[4,1024]{1,0:T(4,128)S(1)}, f32[4,1024]{1,0:T(4,128)S(1)}, f32[1024,4,64]{0,2,1:T(8,128)S(1)})) conditional(s32[]{:T(128)} %clamp.12, (f32[4,1024]{1,0:T(4,128)S(1)}, f32[4,1024]{1,0:T(4,128)S(1)}, f32[1024,4,64]{0,2,1:T(8,128)S(1)}) %tuple.75, (bf16[512,64]{0,1:T(8,128)(2,1)S(1)}, ...), branch_computations={%region_4.4_spmd, %region_5.7_spmd, %region_8.10_spmd} | conditional | flops 577779200 | bytes 30369832 | solution.py:147
  175.5 6.4 %conditional.4 = ((f32[4,1024]{1,0:T(4,128)S(1)}, f32[4,1024]{1,0:T(4,128)S(1)}, f32[1024,4,64]{0,2,1:T(8,128)S(1)})) conditional(s32[]{:T(128)} %clamp.12, (f32[4,1024]{1,0:T(4,128)S(1)}, f32[4,1024]{1,0:T(4,128)S(1)}, f32[1024,4,64]{0,2,1:T(8,128)S(1)}) %tuple.75, (bf16[512,64]{0,1:T(8,128)(2,1)S(1)}, ...), branch_computations={%region_4.4_spmd, %region_5.7_spmd, %region_8.10_spmd} | conditional | flops 577779200 | bytes 30369832 | solution.py:147
  184.5 6.4 %conditional.4 = ((f32[4,1024]{1,0:T(4,128)S(1)}, f32[4,1024]{1,0:T(4,128)S(1)}, f32[1024,4,64]{0,2,1:T(8,128)S(1)})) conditional(s32[]{:T(128)} %clamp.12, (f32[4,1024]{1,0:T(4,128)S(1)}, f32[4,1024]{1,0:T(4,128)S(1)}, f32[1024,4,64]{0,2,1:T(8,128)S(1)}) %tuple.75, (bf16[512,64]{0,1:T(8,128)(2,1)S(1)}, ...), branch_computations={%region_4.4_spmd, %region_5.7_spmd, %region_8.10_spmd} | conditional | flops 577779200 | bytes 30369832 | solution.py:147
  193.6 6.4 %conditional.4 = ((f32[4,1024]{1,0:T(4,128)S(1)}, f32[4,1024]{1,0:T(4,128)S(1)}, f32[1024,4,64]{0,2,1:T(8,128)S(1)})) conditional(s32[]{:T(128)} %clamp.12, (f32[4,1024]{1,0:T(4,128)S(1)}, f32[4,1024]{1,0:T(4,128)S(1)}, f32[1024,4,64]{0,2,1:T(8,128)S(1)}) %tuple.75, (bf16[512,64]{0,1:T(8,128)(2,1)S(1)}, ...), branch_computations={%region_4.4_spmd, %region_5.7_spmd, %region_8.10_spmd} | conditional | flops 577779200 | bytes 30369832 | solution.py:147
  202.7 6.4 %conditional.4 = ((f32[4,1024]{1,0:T(4,128)S(1)}, f32[4,1024]{1,0:T(4,128)S(1)}, f32[1024,4,64]{0,2,1:T(8,128)S(1)})) conditional(s32[]{:T(128)} %clamp.12, (f32[4,1024]{1,0:T(4,128)S(1)}, f32[4,1024]{1,0:T(4,128)S(1)}, f32[1024,4,64]{0,2,1:T(8,128)S(1)}) %tuple.75, (bf16[512,64]{0,1:T(8,128)(2,1)S(1)}, ...), branch_computations={%region_4.4_spmd, %region_5.7_spmd, %region_8.10_spmd} | conditional | flops 577779200 | bytes 30369832 | solution.py:147
  211.8 9.4 %conditional.4 = ((f32[4,1024]{1,0:T(4,128)S(1)}, f32[4,1024]{1,0:T(4,128)S(1)}, f32[1024,4,64]{0,2,1:T(8,128)S(1)})) conditional(s32[]{:T(128)} %clamp.12, (f32[4,1024]{1,0:T(4,128)S(1)}, f32[4,1024]{1,0:T(4,128)S(1)}, f32[1024,4,64]{0,2,1:T(8,128)S(1)}) %tuple.75, (bf16[512,64]{0,1:T(8,128)(2,1)S(1)}, ...), branch_computations={%region_4.4_spmd, %region_5.7_spmd, %region_8.10_spmd} | conditional | flops 577779200 | bytes 30369832 | solution.py:147
  214.6 3.3 %fusion.30 = f32[1024,4,64]{0,2,1:T(8,128)S(1)} fusion(f32[512,1024,4]{1,0,2:T(8,128)S(1)} %get-tuple-element.451, f32[4,1024]{1,0:T(4,128)S(1)} %get-tuple-element.545, f32[4,512]{1,0:T(4,128)S(1)} %get-tuple-element.303, f32[4,1024]{1,0:T(4,128)S(1)} %get-tuple-element.302, pred[1024,512]{0,1:T(8,128)(4,1)S(1)} %broadcast_compare_fusion, ...), kind=kOutput, calls=%fused_computation.27 | convolution fusion | flops 283639808 | bytes 11132928 | tf_op jit(solution)/shard_map/while/body/eval_jaxpr/cond/branch_2_fun/htu,ud->thd/dot_general | solution.py:36
  223.8 9.4 %conditional.4 = ((f32[4,1024]{1,0:T(4,128)S(1)}, f32[4,1024]{1,0:T(4,128)S(1)}, f32[1024,4,64]{0,2,1:T(8,128)S(1)})) conditional(s32[]{:T(128)} %clamp.12, (f32[4,1024]{1,0:T(4,128)S(1)}, f32[4,1024]{1,0:T(4,128)S(1)}, f32[1024,4,64]{0,2,1:T(8,128)S(1)}) %tuple.75, (bf16[512,64]{0,1:T(8,128)(2,1)S(1)}, ...), branch_computations={%region_4.4_spmd, %region_5.7_spmd, %region_8.10_spmd} | conditional | flops 577779200 | bytes 30369832 | solution.py:147
  233.8 11.3 %all_to_all.25 = bf16[4,256,256]{1,2,0:T(8,128)(2,1)S(1)} all-to-all(bf16[4,256,256]{1,2,0:T(8,128)(2,1)S(1)} %copy.52), channel_id=1, replica_groups=mesh['sp'=8,'tp'=4] {'tp'}, dimensions={0} | all-to-all | bytes 1048576 | tf_op jit(solution)/shard_map/all_to_all | solution.py:155
  245.1 4.4 %convolution_convert_fusion = bf16[256,2048]{1,0:T(8,128)(2,1)} fusion(bf16[256,1024]{0,1:T(8,128)(2,1)S(1)} %bitcast.114, bf16[1024,2048]{1,0:T(8,128)(2,1)} %param.22), kind=kOutput, calls=%fused_computation.44 | convolution fusion | flops 1074266112 | bytes 5767168 | tf_op jit(solution)/shard_map/dot_general | solution.py:156
  (253 shorter events, 144.8 us)
Async XLA Ops:
  6.5 1.6 copy-start
  6.5 75.4 %all-gather.2.cloned.1.call-start = ((), (), s32[]{:S(2)}) async-start(), calls=%async_computation.2 | async-start | bytes 2359296 | tf_op jit(solution)/shard_map/all_gather | solution.py:107
  8.1 10.6 %copy-start.3 = (f32[64]{0:T(128)S(1)}, f32[64]{0:T(128)}, u32[]{:S(2)}) copy-start(f32[64]{0:T(128)} %param.19) | copy-start | bytes 772
  8.1 10.7 %copy-start.2 = (f32[64]{0:T(128)S(1)}, f32[64]{0:T(128)}, u32[]{:S(2)}) copy-start(f32[64]{0:T(128)} %param.20) | copy-start | bytes 772
  16.7 18.0 %copy-start.1 = (f32[1024,4]{0,1:T(4,128)S(1)}, f32[1024,4]{0,1:T(4,128)}, u32[]{:S(2)}) copy-start(f32[1024,4]{0,1:T(4,128)} %param.21) | copy-start | bytes 49156
Sparse Core Ops, SparseCore 0:
  34.9 46.9 all-gather.1
